TPU v7x, 32 devices: a whole 2x2x4 slice. The times are simulated.
32 devices in a mesh: sp: 8 (over z, y), tp: 4 (over x, core).
Axes of the slice: x: 2, y: 2, z: 4, core: 2. Of those that a mesh axis runs over, the one named last changes fastest.
Arguments:
- stream: bfloat16 [8192, 2048], P(('sp', 'tp')), may hold values from -6 to 6
- query_rows: bfloat16 [8192, 1024], P('sp', 'tp'), may hold values from -6 to 6
- key_rows: bfloat16 [8192, 1024], P('sp', 'tp'), may hold values from -6 to 6
- value_rows: bfloat16 [8192, 2048], P('sp', 'tp'), may hold values from -6 to 6
- gate_rows: bfloat16 [8192, 2048], P('sp', 'tp'), may hold values from -6 to 6
- log_decay: float32 [8192, 1024], P('sp', 'tp'), may hold values from -1 to 0
- head_gain: float32 [256], replicated, may hold values from 0.1 to 1.9
- out_weight: bfloat16 [2048, 2048], P('tp'), may hold values from -0.125 to 0.125
- mix_gain: float32 [2048], replicated, may hold values from 0.1 to 1.9
- up_weight: bfloat16 [2048, 8192], P('sp', 'tp'), may hold values from -0.125 to 0.125
- down_weight: bfloat16 [2048, 8192], P('sp', 'tp'), may hold values from -0.0625 to 0.0625
Outputs:
- mixed_out: bfloat16 [8192, 2048], P(('sp', 'tp'))
All inputs are finite; a program needn't handle non-finite values.
Results may differ from a plain program's by a relative error of at most 0.02.
Values may be sent and summed in bfloat16 or wider, within the bound.
A program may use at most 128 MiB of HBM per device.

v0:
```python
import jax
import jax.numpy as jnp
from jax import lax
from jax.sharding import PartitionSpec as P

KEY_CHANNELS = 128
DV = 256
BLOCK = 64
EPS = 1e-06


def prefix(shard, axis, join, neutral):
    place = lax.axis_index(axis)
    gathered = jax.tree.map(
        lambda a, kind: lax.all_gather(a.astype(kind), axis), shard, (jnp.bfloat16, jnp.bfloat16)
    )
    state = jax.tree.map(lambda a, e: jnp.zeros_like(a) + jnp.asarray(e, a.dtype), shard, neutral)

    def one(step, state):
        return join(
            state,
            jax.tree.map(
                lambda a, own: lax.dynamic_index_in_dim(a, step, 0, False).astype(own.dtype),
                gathered,
                shard,
            ),
        )

    return lax.fori_loop(0, place, one, state)


def chain(earlier, later):
    return (earlier[0] * later[0], later[0][..., None] * earlier[1] + later[1])


def squared_relu(pre):
    return jnp.square(jax.nn.relu(pre)).astype(jnp.bfloat16)


def local(
    stream,
    query_rows,
    key_rows,
    value_rows,
    gate_rows,
    log_decay,
    head_gain,
    out_weight,
    mix_gain,
    up_weight,
    down_weight,
):
    rows = query_rows.shape[0]
    heads_here = query_rows.shape[1] // KEY_CHANNELS
    count = rows // BLOCK
    queries = query_rows.astype(jnp.float32).reshape(
        count, BLOCK, heads_here, KEY_CHANNELS
    ) * KEY_CHANNELS ** (-0.5)
    keys_all = key_rows.astype(jnp.float32).reshape(count, BLOCK, heads_here, KEY_CHANNELS)
    values_all = value_rows.astype(jnp.float32).reshape(count, BLOCK, heads_here, DV)
    decay_rates = log_decay.reshape(count, BLOCK, heads_here, KEY_CHANNELS)
    cum = jnp.cumsum(decay_rates, axis=1)
    last = cum[:, -1:]
    decayed_state = keys_all * jnp.exp(last - cum)
    state_updates = jnp.einsum(
        "nshk,nshv->nhkv", decayed_state, values_all, precision=lax.Precision.HIGHEST
    )
    end_log = last[:, 0]
    total_log = jnp.cumsum(end_log, axis=0)
    tail_weights = jnp.exp(total_log[-1] - total_log)
    summary_state = jnp.einsum(
        "mfa,mfaq->faq", tail_weights, state_updates, precision=lax.Precision.HIGHEST
    )
    summary_decay = jnp.exp(total_log[-1])
    incoming = prefix(
        (summary_decay, summary_state),
        "sp",
        chain,
        (jnp.ones_like(summary_decay), jnp.zeros_like(summary_state)),
    )

    def step(matrix_state, inputs):
        factor, state_update, query_block = inputs
        matrix_state = factor[..., None] * matrix_state + state_update
        head_output = jnp.einsum(
            "wle,leg->wlg", query_block, matrix_state, precision=lax.Precision.HIGHEST
        )
        return (matrix_state, head_output)

    _, outs = lax.scan(step, incoming[1], (jnp.exp(end_log), state_updates, queries))
    readout = outs.reshape(rows, heads_here, DV)
    scaled = readout * lax.rsqrt(jnp.mean(readout * readout, axis=-1, keepdims=True) + EPS)
    gates = gate_rows.astype(jnp.float32).reshape(rows, heads_here, DV)
    gated = scaled * head_gain * jax.nn.silu(gates)
    heads_out = gated.reshape(rows, heads_here * DV).astype(jnp.bfloat16)
    whole_weight = lax.all_gather(out_weight, "tp", axis=0, tiled=True)
    mine = lax.all_to_all(heads_out, "tp", split_axis=0, concat_axis=1, tiled=True)
    attn = jnp.dot(mine, whole_weight, preferred_element_type=jnp.float32)
    midf = (stream.astype(jnp.float32) + attn).astype(jnp.bfloat16).astype(jnp.float32)
    normed = (
        midf * lax.rsqrt(jnp.mean(midf * midf, axis=-1, keepdims=True) + EPS) * mix_gain
    ).astype(jnp.bfloat16)
    gathered = lax.all_gather(normed, "tp", axis=0, tiled=True)
    pre = jnp.dot(
        gathered,
        lax.all_gather(up_weight, "sp", axis=0, tiled=True),
        preferred_element_type=jnp.float32,
    )
    hidden = squared_relu(pre)
    down_full = lax.all_gather(down_weight, "sp", axis=0, tiled=True)
    feed = lax.psum_scatter(
        lax.dot_general(
            hidden, down_full, (((1,), (1,)), ((), ())), preferred_element_type=jnp.float32
        ).astype(jnp.bfloat16),
        "tp",
        scatter_dimension=0,
        tiled=True,
    ).astype(jnp.float32)
    return (midf + feed).astype(jnp.bfloat16)


def solution(mesh):
    placed = (
        P(("sp", "tp"), None),
        P("sp", "tp"),
        P("sp", "tp"),
        P("sp", "tp"),
        P("sp", "tp"),
        P("sp", "tp"),
        P(),
        P("tp", None),
        P(),
        P("sp", "tp"),
        P("sp", "tp"),
    )
    return jax.shard_map(
        local, mesh=mesh, in_specs=placed, out_specs=P(("sp", "tp"), None), check_vma=False
    )
```

profile of v0, /device:TPU:0, one launch (start us, length us, event | category | flops | bytes accessed | tf_op | source)
XLA Modules:
  0.0 489.8 jit_solution(16888176910479370243)
XLA Ops:
  6.5 1.8 reshape.64
  9.1 1.6 reshape.72
  11.4 1.3 reshape.67
  12.7 2.0 fusion.13
  14.8 4.6 fusion.1
  22.2 22.3 %all_gather.22 = bf16[8,2,128]{2,1,0:T(2,128)(2,1)S(1)} all-gather(bf16[1,2,128]{2,1,0:T(2,128)(2,1)S(1)} %get-tuple-element.136), channel_id=1, replica_groups=mesh['sp'=8,'tp'=4] {'sp'}, dimensions={0}, use_global_device_ids=true | all-gather | bytes 4608 | tf_op jit(solution)/shard_map/all_gather | solution.py:15
  44.5 1.1 convert_multiply_fusion.3
  45.6 1.5 mul.94
  47.1 16.1 %all-gather.15.cloned.1.call-done = bf16[16,128,256]{2,1,0:T(8,128)(2,1)} async-done(((bf16[2,128,256]{2,1,0:T(8,128)(2,1)}), bf16[16,128,256]{2,1,0:T(8,128)(2,1)}) %all-gather.15.cloned.1.call-update) | async-done | bytes 1048592 | tf_op jit(solution)/shard_map/all_gather | solution.py:15
  63.4 36.3 %while.25 = (s32[]{:T(128)}, f32[2,128,256]{2,1,0:T(8,128)S(1)}, f32[16,64,2,256]{3,1,2,0:T(8,128)S(1)}, f32[16,2,128]{2,0,1:T(8,128)S(1)}, f32[16,2,128,256]{3,...) while((s32[]{:T(128)}, f32[2,128,256]{2,1,0:T(8,128)S(1)}, f32[16,64,2,256]{3,1,2,0:T(8,128)S(1)}, ...), condition=%wide.region_5.6_spmd, body=%wide.region_4.5_spmd.sunk | while | flops 50462720 | bytes 1379421 | solution.py:90
  63.5 1.1 bitcast_add_fusion.2
  65.7 1.1 bitcast_add_fusion.2
  68.0 1.1 bitcast_add_fusion.2
  70.2 1.1 bitcast_add_fusion.2
  72.6 1.1 bitcast_add_fusion.2
  74.9 1.1 bitcast_add_fusion.2
  79.4 1.1 bitcast_add_fusion.2
  81.7 1.1 bitcast_add_fusion.2
  86.2 1.1 bitcast_add_fusion.2
  93.0 1.1 bitcast_add_fusion.2
  99.7 3.0 copy.53
  103.4 1.2 mul.96
  104.8 1.4 copy-done.3
  108.7 22.5 %all_to_all.19 = bf16[4,256,512]{1,2,0:T(8,128)(2,1)S(1)} all-to-all(bf16[4,256,512]{1,2,0:T(8,128)(2,1)S(1)} %copy.56), channel_id=1, replica_groups=mesh['sp'=8,'tp'=4] {'tp'}, dimensions={0} | all-to-all | bytes 2097152 | tf_op jit(solution)/shard_map/all_to_all | solution.py:97
  131.2 6.5 %fusion.8 = (f32[256]{0:T(256)S(1)}, bf16[256,2048]{1,0:T(8,128)(2,1)S(1)}) fusion(bf16[256,2048]{0,1:T(8,128)(2,1)S(1)} %bitcast.70, bf16[2048,2048]{1,0:T(8,128)(2,1)} %all-gather.7.cloned.1.call-done, bf16[256,2048]{1,0:T(8,128)(2,1)} %param.15), kind=kOutput, calls=%fused_computation.23 | convolution fusion | flops 2150629120 | bytes 11535360 | tf_op jit(solution)/shard_map/dot_general | solution.py:98
  137.7 1.3 fusion.10
  139.3 112.1 %all-gather.11.cloned.1.call-done = bf16[2048,2048]{1,0:T(8,128)(2,1)} async-done(((bf16[256,2048]{1,0:T(8,128)(2,1)}), bf16[2048,2048]{1,0:T(8,128)(2,1)}) %all-gather.11.cloned.1.call-update) | async-done | bytes 8388624 | tf_op jit(solution)/shard_map/all_gather | solution.py:106
  251.4 124.7 %all-gather.13.cloned.1.call-done = bf16[2048,2048]{1,0:T(8,128)(2,1)} async-done(((bf16[256,2048]{1,0:T(8,128)(2,1)}), bf16[2048,2048]{1,0:T(8,128)(2,1)}) %all-gather.13.cloned.1.call-update) | async-done | bytes 8388624 | tf_op jit(solution)/shard_map/all_gather | solution.py:110
  376.1 34.1 %all-gather.9.cloned.1.call-done = bf16[1024,2048]{1,0:T(8,128)(2,1)} async-done(((bf16[256,2048]{1,0:T(8,128)(2,1)}), bf16[1024,2048]{1,0:T(8,128)(2,1)}) %all-gather.9.cloned.1.call-update) | async-done | bytes 4194320 | tf_op jit(solution)/shard_map/all_gather | solution.py:103
  410.2 25.4 %convolution_convert_fusion = bf16[1024,2048]{1,0:T(8,128)(2,1)} fusion(bf16[2048,2048]{1,0:T(8,128)(2,1)} %all-gather.13.cloned.1.call-done, bf16[1024,2048]{1,0:T(8,128)(2,1)} %all-gather.9.cloned.1.call-done, bf16[2048,2048]{1,0:T(8,128)(2,1)} %all-gather.11.cloned.1.call-done), kind=kOutput, calls=%fused_computation.11 | convolution fusion | flops 17188257792 | bytes 25165824 | tf_op jit(solution)/shard_map/dot_general | solution.py:112
  435.6 44.7 %reduce-scatter.2.cloned.1.call-done = bf16[256,2048]{1,0:T(8,128)(2,1)} async-done(((bf16[1024,2048]{1,0:T(8,128)(2,1)}), bf16[256,2048]{1,0:T(8,128)(2,1)}) %reduce-scatter.2.cloned.1.call-update) | async-done | bytes 1048592 | tf_op jit(solution)/shard_map/reduce_scatter | solution.py:111
  480.3 2.6 fusion.11
  (100 shorter events, 32.9 us)
Async XLA Ops:
  6.5 40.6 %copy-start = (f32[256]{0:T(256)S(1)}, f32[256]{0:T(256)}, u32[]{:S(2)}) copy-start(f32[256]{0:T(256)} %param.21) | copy-start | bytes 3076
  6.5 56.7 %all-gather.15.cloned.1.call-start = ((), (), s32[]{:S(2)}) async-start(), calls=%async_computation.7 | async-start | bytes 1179648 | tf_op jit(solution)/shard_map/all_gather | solution.py:15
  14.7 4.6 copy-start.2
  20.1 111.2 %all-gather.7.cloned.1.call-start = ((), (), s32[]{:S(2)}) async-start(), calls=%async_computation.2 | async-start | bytes 10485760 | tf_op jit(solution)/shard_map/all_gather | solution.py:96
  20.8 230.6 %all-gather.11.cloned.1.call-start = ((), (), s32[]{:S(2)}) async-start(), calls=%async_computation.4 | async-start | bytes 9437184 | tf_op jit(solution)/shard_map/all_gather | solution.py:106
  21.5 354.6 %all-gather.13.cloned.1.call-start = ((), (), s32[]{:S(2)}) async-start(), calls=%async_computation.5 | async-start | bytes 9437184 | tf_op jit(solution)/shard_map/all_gather | solution.py:110
  22.1 388.1 %all-gather.9.cloned.1.call-start = ((), (), s32[]{:S(2)}) async-start(), calls=%async_computation.3 | async-start | bytes 5242880 | tf_op jit(solution)/shard_map/all_gather | solution.py:103
  104.6 1.6 copy-start.3
  106.2 1.2 copy-start.4
  131.2 6.5 %copy-start.5 = (f32[2048]{0:T(1024)S(1)}, f32[2048]{0:T(1024)}, u32[]{:S(2)}) copy-start(f32[2048]{0:T(1024)} %param.23) | copy-start | bytes 24580
  139.0 341.3 %reduce-scatter.2.cloned.1.call-start = ((), (), s32[]{:S(2)}) async-start(), calls=%async_computation.6 | async-start | bytes 5242880 | tf_op jit(solution)/shard_map/reduce_scatter | solution.py:111
  435.6 47.3 %copy-start.1 = (f32[256]{0:T(256)S(1)}, f32[256]{0:T(256)}, u32[]{:S(2)}) copy-start(f32[256]{0:T(256)} %param.21) | copy-start | bytes 3076
Sparse Core Ops, SparseCore 0:
  20.2 42.9 all-gather.14
  64.8 62.6 all-gather.6
  129.6 121.8 all-gather.10
  253.4 122.6 all-gather.12
  377.5 32.6 all-gather.8
  435.7 44.5 reduce-scatter.1
where the time goes:
time: 492 us; the launch traced here: 490 us
  waiting for transfers between devices  334 us (68%)
  blocking collectives  44.8 us (9%)
  matrix products  43.1 us (9%)
  local copies, waits for them, and re-layouts  28.6 us (6%)
  other arithmetic  24.7 us (5%)
  between operations  13.7 us (3%)
    all_gather x1, waiting for transfers between devices, local(): down_full = lax.all_gather(down_weight, 'sp', axis=0, tiled=True)  125 us
    all_gather x1, waiting for transfers between devices, local(): lax.all_gather(up_weight, 'sp', axis=0, tiled=True)  112 us
    reduce_scatter x1, waiting for transfers between devices, local(): lax.psum_scatter(lax.dot_general(hidden, down_full, (((1,), (1,)), ((), (...  44.7 us
    all_gather x1, waiting for transfers between devices, local(): gathered = lax.all_gather(normed, 'tp', axis=0, tiled=True)  34.1 us
    dot_general x1, matrix products, local(): lax.dot_general(hidden, down_full, (((1,), (1,)), ((), ())), preferred_el...  25.4 us
    all_to_all x1, blocking collectives, local(): lax.all_to_all(heads_out, 'tp', split_axis=0, concat_axis=1, tiled=True)  22.5 us
    all_gather x1, blocking collectives, prefix(): lax.all_gather(a.astype(kind), axis)  22.3 us
    add x16, other arithmetic, step(): matrix_state = factor[..., None] * matrix_state + state_update  17.2 us
  transfers between devices with their start and end apart: 6, of which 5 were waited for; matrix products, arithmetic and copies ran while one was open for 11% of the time, Pallas kernels for 0%

commit v1 on v0

--- a/solution.py
+++ b/solution.py
@@ -100,7 +100,13 @@
     normed = (
         midf * lax.rsqrt(jnp.mean(midf * midf, axis=-1, keepdims=True) + EPS) * mix_gain
     ).astype(jnp.bfloat16)
-    gathered = lax.all_gather(normed, "tp", axis=0, tiled=True)
+    devices = lax.axis_size("tp")
+    held, blocks = (normed, [normed])
+    for _ in range(devices - 1):
+        held = lax.ppermute(held, "tp", [(i, (i + 1) % devices) for i in range(devices)])
+        blocks.insert(0, held)
+    line = jnp.concatenate(blocks, axis=0)
+    gathered = jnp.roll(line, (lax.axis_index("tp") + 1) * normed.shape[0], axis=0)
     pre = jnp.dot(
         gathered,
         lax.all_gather(up_weight, "sp", axis=0, tiled=True),

time: 492 us -> 459 us (0.933)
  waiting for transfers between devices: 334 us -> 289 us
  local copies, waits for them, and re-layouts: 28.6 us -> 37.9 us
    all_gather x1, waiting for transfers between devices: 125 us -> 60.9 us  [local(): down_full = lax.all_gather(down_weight, 'sp', axis=0, tiled=True)]
    ppermute x0 -> x3, waiting for transfers between devices: none -> 42.8 us  [local(): lax.ppermute(held, 'tp', [(i, (i + 1) % devices) for i in range(devices)])]
    all_gather x1 -> x0, waiting for transfers between devices: 34.1 us -> none  [local(): gathered = lax.all_gather(normed, 'tp', axis=0, tiled=True)]
    all_gather x1, waiting for transfers between devices: 112 us -> 125 us  [local(): lax.all_gather(up_weight, 'sp', axis=0, tiled=True)]
    unnamed x16 -> x22, local copies, waits for them, and re-layouts: 2.82 us -> 12.2 us
  transfers between devices with their start and end apart: 6 -> 8, of which waited for: 5 -> 7; matrix products, arithmetic and copies ran while one was open for 11% -> 14% of each run, Pallas kernels for 0% -> 0%
where the time goes in v1:
time: 459 us; the launch traced here: 457 us
  waiting for transfers between devices  289 us (63%)
  blocking collectives  46.4 us (10%)
  matrix products  42.7 us (9%)
  local copies, waits for them, and re-layouts  37.9 us (8%)
  other arithmetic  26.4 us (6%)
  between operations  13.4 us (3%)
    all_gather x1, waiting for transfers between devices, local(): lax.all_gather(up_weight, 'sp', axis=0, tiled=True)  125 us
    all_gather x1, waiting for transfers between devices, local(): down_full = lax.all_gather(down_weight, 'sp', axis=0, tiled=True)  60.9 us
    reduce_scatter x1, waiting for transfers between devices, local(): lax.psum_scatter(lax.dot_general(hidden, down_full, (((1,), (1,)), ((), (...  42.9 us
    ppermute x3, waiting for transfers between devices, local(): lax.ppermute(held, 'tp', [(i, (i + 1) % devices) for i in range(devices)])  42.8 us
    dot_general x1, matrix products, local(): lax.dot_general(hidden, down_full, (((1,), (1,)), ((), ())), preferred_el...  25.4 us
    all_to_all x1, blocking collectives, local(): lax.all_to_all(heads_out, 'tp', split_axis=0, concat_axis=1, tiled=True)  24.1 us
    all_gather x1, blocking collectives, prefix(): lax.all_gather(a.astype(kind), axis)  22.3 us
    add x16, other arithmetic, step(): matrix_state = factor[..., None] * matrix_state + state_update  17.2 us
  transfers between devices with their start and end apart: 8, of which 7 were waited for; matrix products, arithmetic and copies ran while one was open for 14% of the time, Pallas kernels for 0%

profile of v1, /device:TPU:0, one launch (start us, length us, event | category | flops | bytes accessed | tf_op | source)
XLA Modules:
  0.0 457.1 jit_solution(16293838050907203109)
XLA Ops:
  6.5 1.8 reshape.64
  9.1 1.6 reshape.72
  11.4 1.3 reshape.67
  12.7 2.0 fusion.20
  14.8 2.0 copy-done.2
  16.7 4.6 %fusion.1 = bf16[2,128,1,256]{3,2,1,0:T(2,128)(2,1)S(1)} fusion(f32[16,2,128,1]{0,3,2,1:T(1,128)S(1)} %copy.57, f32[16,2,128,256]{3,2,1,0:T(8,128)S(1)} %fusion.20), kind=kOutput, calls=%fused_computation.9 | convolution fusion | flops 12582912 | bytes 4341760 | tf_op jit(solution)/shard_map/mfa,mfaq->faq/dot_general | solution.py:71
  24.1 22.3 %all_gather.19 = bf16[8,2,128]{2,1,0:T(2,128)(2,1)S(1)} all-gather(bf16[1,2,128]{2,1,0:T(2,128)(2,1)S(1)} %get-tuple-element.136), channel_id=1, replica_groups=mesh['sp'=8,'tp'=4] {'sp'}, dimensions={0}, use_global_device_ids=true | all-gather | bytes 4608 | tf_op jit(solution)/shard_map/all_gather | solution.py:15
  46.5 1.1 convert_multiply_fusion.3
  47.6 1.5 mul.97
  49.1 16.1 %all-gather.12.cloned.1.call-done = bf16[16,128,256]{2,1,0:T(8,128)(2,1)} async-done(((bf16[2,128,256]{2,1,0:T(8,128)(2,1)}), bf16[16,128,256]{2,1,0:T(8,128)(2,1)}) %all-gather.12.cloned.1.call-update) | async-done | bytes 1048592 | tf_op jit(solution)/shard_map/all_gather | solution.py:15
  65.4 36.2 %while.25 = (s32[]{:T(128)}, f32[2,128,256]{2,1,0:T(8,128)S(1)}, f32[16,64,2,256]{3,1,2,0:T(8,128)S(1)}, f32[16,2,128]{2,0,1:T(8,128)S(1)}, f32[16,2,128,256]{3,...) while((s32[]{:T(128)}, f32[2,128,256]{2,1,0:T(8,128)S(1)}, f32[16,64,2,256]{3,1,2,0:T(8,128)S(1)}, ...), condition=%wide.region_5.6_spmd, body=%wide.region_4.5_spmd.sunk | while | flops 50462720 | bytes 1379421 | solution.py:90
  72.2 1.1 bitcast_add_fusion.2
  74.5 1.1 bitcast_add_fusion.2
  76.8 1.1 bitcast_add_fusion.2
  83.6 1.1 bitcast_add_fusion.2
  94.9 1.1 bitcast_add_fusion.2
  101.6 3.0 copy.53
  105.3 1.2 mul.99
  109.1 24.1 %all_to_all.19 = bf16[4,256,512]{1,2,0:T(8,128)(2,1)S(1)} all-to-all(bf16[4,256,512]{1,2,0:T(8,128)(2,1)S(1)} %copy.56), channel_id=1, replica_groups=mesh['sp'=8,'tp'=4] {'tp'}, dimensions={0} | all-to-all | bytes 2097152 | tf_op jit(solution)/shard_map/all_to_all | solution.py:97
  133.2 6.1 %fusion.15 = (f32[256]{0:T(256)S(1)}, bf16[256,2048]{1,0:T(8,128)(2,1)S(1)}) fusion(bf16[256,2048]{0,1:T(8,128)(2,1)S(1)} %bitcast.69, bf16[2048,2048]{1,0:T(8,128)(2,1)} %all-gather.6.cloned.1.call-done, bf16[256,2048]{1,0:T(8,128)(2,1)} %param.15), kind=kOutput, calls=%fused_computation.25 | convolution fusion | flops 2150629120 | bytes 11535360 | tf_op jit(solution)/shard_map/dot_general | solution.py:98
  139.7 14.2 %collective-permute-done = bf16[256,2048]{1,0:T(8,128)(2,1)S(1)} collective-permute-done((bf16[256,2048]{1,0:T(8,128)(2,1)S(1)}, bf16[256,2048]{1,0:T(8,128)(2,1)S(1)}, u32[]{:S(2)}, u32[]{:S(2)}) %collective-permute-start) | collective-permute-done | bytes 1048608 | tf_op jit(solution)/shard_map/ppermute | solution.py:106
  153.9 14.2 %collective-permute-done.1 = bf16[256,2048]{1,0:T(8,128)(2,1)S(1)} collective-permute-done((bf16[256,2048]{1,0:T(8,128)(2,1)S(1)}, bf16[256,2048]{1,0:T(8,128)(2,1)S(1)}, u32[]{:S(2)}, u32[]{:S(2)}) %collective-permute-start.1) | collective-permute-done | bytes 1048608 | tf_op jit(solution)/shard_map/ppermute | solution.py:106
  168.1 14.3 %collective-permute-done.2 = bf16[256,2048]{1,0:T(8,128)(2,1)} collective-permute-done((bf16[256,2048]{1,0:T(8,128)(2,1)S(1)}, bf16[256,2048]{1,0:T(8,128)(2,1)}, u32[]{:S(2)}, u32[]{:S(2)}) %collective-permute-start.2) | collective-permute-done | bytes 1048608 | tf_op jit(solution)/shard_map/ppermute | solution.py:106
  182.5 2.4 constant_dynamic-update-slice_fusion.7
  187.0 1.3 constant_dynamic-update-slice_fusion.4
  188.3 2.3 constant_dynamic-update-slice_fusion.3
  192.7 1.3 constant_dynamic-update-slice_fusion
  194.0 60.9 %all-gather.10.cloned.1.call-done = bf16[2048,2048]{1,0:T(8,128)(2,1)} async-done(((bf16[256,2048]{1,0:T(8,128)(2,1)}), bf16[2048,2048]{1,0:T(8,128)(2,1)}) %all-gather.10.cloned.1.call-update) | async-done | bytes 8388624 | tf_op jit(solution)/shard_map/all_gather | solution.py:116
  255.0 124.7 %all-gather.8.cloned.1.call-done = bf16[2048,2048]{1,0:T(8,128)(2,1)} async-done(((bf16[256,2048]{1,0:T(8,128)(2,1)}), bf16[2048,2048]{1,0:T(8,128)(2,1)}) %all-gather.8.cloned.1.call-update) | async-done | bytes 8388624 | tf_op jit(solution)/shard_map/all_gather | solution.py:112
  379.6 25.4 %fusion.7 = bf16[1024,2048]{1,0:T(8,128)(2,1)} fusion(bf16[2048,2048]{1,0:T(8,128)(2,1)} %all-gather.10.cloned.1.call-done, bf16[2048,2048]{1,0:T(8,128)(2,1)} %all-gather.8.cloned.1.call-done, bf16[2048,2048]{1,0:T(8,128)(2,1)} %constant_dynamic-update-slice_fusion, s32[]{:T(128)S(6)} %select_n.21), kind=kOutput, calls=%fused_computation.13 | convolution fusion | flops 17188257792 | bytes 25165828 | tf_op jit(solution)/shard_map/dot_general | solution.py:118
  405.1 42.9 %reduce-scatter.2.cloned.1.call-done = bf16[256,2048]{1,0:T(8,128)(2,1)} async-done(((bf16[1024,2048]{1,0:T(8,128)(2,1)}), bf16[256,2048]{1,0:T(8,128)(2,1)}) %reduce-scatter.2.cloned.1.call-update) | async-done | bytes 1048592 | tf_op jit(solution)/shard_map/reduce_scatter | solution.py:117
  448.0 2.6 fusion.18
  (111 shorter events, 42.4 us)
Async XLA Ops:
  6.5 42.5 %copy-start = (f32[256]{0:T(256)S(1)}, f32[256]{0:T(256)}, u32[]{:S(2)}) copy-start(f32[256]{0:T(256)} %param.21) | copy-start | bytes 3076
  6.5 58.6 %all-gather.12.cloned.1.call-start = ((), (), s32[]{:S(2)}) async-start(), calls=%async_computation.6 | async-start | bytes 1179648 | tf_op jit(solution)/shard_map/all_gather | solution.py:15
  14.7 2.0 copy-start.2
  22.0 111.2 %all-gather.6.cloned.1.call-start = ((), (), s32[]{:S(2)}) async-start(), calls=%async_computation.2 | async-start | bytes 10485760 | tf_op jit(solution)/shard_map/all_gather | solution.py:96
  22.8 232.2 %all-gather.10.cloned.1.call-start = ((), (), s32[]{:S(2)}) async-start(), calls=%async_computation.4 | async-start | bytes 9437184 | tf_op jit(solution)/shard_map/all_gather | solution.py:116
  23.5 356.1 %all-gather.8.cloned.1.call-start = ((), (), s32[]{:S(2)}) async-start(), calls=%async_computation.3 | async-start | bytes 9437184 | tf_op jit(solution)/shard_map/all_gather | solution.py:112
  24.1 423.9 %reduce-scatter.2.cloned.1.call-start = ((), (), s32[]{:S(2)}) async-start(), calls=%async_computation.5 | async-start | bytes 5242880 | tf_op jit(solution)/shard_map/reduce_scatter | solution.py:117
  105.0 1.7 copy-start.3
  106.5 1.2 copy-start.4
  133.2 6.1 %copy-start.5 = (f32[2048]{0:T(1024)S(1)}, f32[2048]{0:T(1024)}, u32[]{:S(2)}) copy-start(f32[2048]{0:T(1024)} %param.23) | copy-start | bytes 24580
  139.6 14.3 %collective-permute-start = (bf16[256,2048]{1,0:T(8,128)(2,1)S(1)}, bf16[256,2048]{1,0:T(8,128)(2,1)S(1)}, u32[]{:S(2)}, u32[]{:S(2)}) collective-permute-start(bf16[256,2048]{1,0:T(8,128)(2,1)S(1)} %fusion.17), channel_id=1, source_target_pairs={{0,1},{1,2},{2,3},{3,0},{4,5},{5,6},{6,7},{7,4},{8,9},{9,10},{10,1... | collective-permute-start | bytes 3145736 | tf_op jit(solution)/shard_map/ppermute | solution.py:106
  153.9 14.2 %collective-permute-start.1 = (bf16[256,2048]{1,0:T(8,128)(2,1)S(1)}, bf16[256,2048]{1,0:T(8,128)(2,1)S(1)}, u32[]{:S(2)}, u32[]{:S(2)}) collective-permute-start(bf16[256,2048]{1,0:T(8,128)(2,1)S(1)} %collective-permute-done), channel_id=1, source_target_pairs={{0,1},{1,2},{2,3},{3,0},{4,5},{5,6},{6,7},{7,4},{8,9},{9,10},{10,1... | collective-permute-start | bytes 3145736 | tf_op jit(solution)/shard_map/ppermute | solution.py:106
  168.1 14.3 %collective-permute-start.2 = (bf16[256,2048]{1,0:T(8,128)(2,1)S(1)}, bf16[256,2048]{1,0:T(8,128)(2,1)}, u32[]{:S(2)}, u32[]{:S(2)}) collective-permute-start(bf16[256,2048]{1,0:T(8,128)(2,1)S(1)} %collective-permute-done.1), channel_id=1, source_target_pairs={{0,1},{1,2},{2,3},{3,0},{4,5},{5,6},{6,7},{7,4},{8,9},{9,10},{10,1... | collective-permute-start | bytes 3145736 | tf_op jit(solution)/shard_map/ppermute | solution.py:106
  379.6 70.9 %copy-start.1 = (f32[256]{0:T(256)S(1)}, f32[256]{0:T(256)}, u32[]{:S(2)}) copy-start(f32[256]{0:T(256)} %param.21) | copy-start | bytes 3076
Sparse Core Ops, SparseCore 0:
  22.1 42.9 all-gather.11
  66.7 64.1 all-gather.5
  133.1 121.8 all-gather.9
  256.9 122.6 all-gather.7
  405.2 42.7 reduce-scatter.1
